TPU v7x, 512 devices: a whole 4x8x8 slice. The times are simulated.
512 devices in a mesh: gr: 2 (over z_hi), fs: 32 (over z_lo, y), tp: 8 (over x, core).
Axes of the slice: x: 4, y: 8, z: 8 (z_hi: 2, z_lo: 4; z = z_hi * 4 + z_lo), core: 2. Of those that a mesh axis runs over, the one named last changes fastest.
Arguments:
- prompt: bfloat16 [20480, 2048], P(('gr', 'fs'), 'tp'), may hold values from -6 to 6
- norm_gain: float32 [2048], P(('gr', 'fs')), may hold values from 0.1 to 1.9
- gate_weight: float32 [32, 2048, 2048], P(None, ('gr', 'fs'), 'tp'), may hold values from -0.125 to 0.125
- up_weight: float32 [32, 2048, 2048], P(None, ('gr', 'fs'), 'tp'), may hold values from -0.125 to 0.125
- down_weight: float32 [32, 2048, 2048], P(None, ('gr', 'fs'), 'tp'), may hold values from -0.125 to 0.125
- routes: int32 [20480, 2], P(('gr', 'fs')), may hold values from 0 to 31, as said below
- route_weight: float32 [20480, 2], P(('gr', 'fs')), may hold values from 0.2 to 1
Outputs:
- gate_new: bfloat16 [32, 2048, 2048], P('fs', None, 'tp')
- up_new: bfloat16 [32, 2048, 2048], P('fs', None, 'tp')
- down_new: bfloat16 [32, 2048, 2048], P('fs', 'tp')
- mixed: bfloat16 [20480, 2048], P(('gr', 'fs'), 'tp')
Inputs may be any that keep to these rules, and one draw needn't show every extreme that they name: `routes`: each row names two different experts of the same group; expert e belongs to group e // 8. Among the 320 rows of one index of gr and fs no expert is named more than 30 times, and in every draw every expert of one group is named exactly 30 times by the rows of every index.
All inputs are finite; a program needn't handle non-finite values.
Results may differ from a plain program's by a relative error of at most 0.015.
Values may be sent and summed in bfloat16 or wider, within the bound.
No kernel may reach another device: no remote copies, remote signals or barrier semaphores. Data moves between devices by JAX's collectives and lax.ppermute only.
A program may use at most 64 MiB of HBM per device.

v0:
```python
import jax
import jax.numpy as jnp
from jax import lax
from jax.sharding import PartitionSpec as P

CAP = 30


def side_by_side(arrays, axis, split_dim, concat_dim, along):
    widths = [a.shape[along] for a in arrays]
    both = jnp.concatenate(arrays, axis=along)
    whole = lax.all_to_all(both, axis, split_axis=split_dim, concat_axis=concat_dim, tiled=True)
    return tuple(jnp.split(whole, [sum(widths[:k]) for k in range(1, len(widths))], axis=along))


def side_by_side_2(arrays, axis, dim, along):
    ends, at = ([], 0)
    for a in arrays[:-1]:
        at += a.shape[along]
        ends.append(at)
    both = jnp.concatenate(arrays, axis=along)
    return tuple(jnp.split(lax.all_gather(both, axis, axis=dim, tiled=True), ends, axis=along))


def copy_for_each(array, axis):
    length = lax.axis_size(axis)
    return lax.all_to_all(
        jnp.broadcast_to(array[None], (length, *array.shape)), axis, 0, 0, tiled=True
    )


def over_copies(array, axis):
    everything = copy_for_each(array, axis)
    return jnp.sum(everything, axis=0)


def body(prompt, norm_gain, gate_weight, up_weight, down_weight, routes, route_weight):
    groups_fs = lax.axis_size("fs")
    groups_tp = lax.axis_size("tp")
    gate_cast = (gate_weight * norm_gain[None, :, None]).astype(jnp.bfloat16)
    up_cast = (up_weight * norm_gain[None, :, None]).astype(jnp.bfloat16)
    down_cast = down_weight.astype(jnp.bfloat16)
    spread = side_by_side((gate_cast, up_cast, down_cast), "fs", 0, 1, 2)
    gate_new, up_new, down_rows = side_by_side_2((spread[0], spread[1], spread[2]), "gr", 1, 0)
    down_new = lax.all_to_all(down_rows, "tp", split_axis=1, concat_axis=2, tiled=True)
    values = prompt.astype(jnp.float32)
    tok_count = prompt.shape[0]
    col_width = prompt.shape[1]
    full_width = col_width * groups_tp
    squares = jnp.sum(values * values, axis=-1, keepdims=True)
    total_squares = over_copies(squares, "tp")
    normed = (values * lax.rsqrt(total_squares / full_width + 1e-06)).astype(jnp.bfloat16)
    expert_total = gate_weight.shape[0]
    per_device = expert_total // groups_fs
    slots_all = expert_total * CAP
    picks_flat = routes.reshape(-1)
    matches = (picks_flat[:, None] == jnp.arange(expert_total, dtype=jnp.int32)[None, :]).astype(
        jnp.int32
    )
    earlier = jnp.cumsum(matches, axis=0) - matches
    slot_of = jnp.sum(earlier * matches, axis=1)
    target = (picks_flat * CAP + slot_of).reshape(tok_count, 2)
    slot_ids = jnp.arange(slots_all, dtype=jnp.int32)[None, :]
    select_first = (target[:, 0:1] == slot_ids).astype(jnp.bfloat16)
    select_second = (target[:, 1:2] == slot_ids).astype(jnp.bfloat16)
    select_both = select_first + select_second
    outbound = jnp.einsum("ts,td->sd", select_both, normed, preferred_element_type=jnp.float32)
    outbound = outbound.astype(jnp.bfloat16).reshape(groups_fs, per_device, CAP, col_width)
    moved_cols = lax.all_to_all(outbound, "fs", split_axis=0, concat_axis=0, tiled=True)
    arrived_rows = lax.all_gather(moved_cols, "tp", axis=3, tiled=True)
    gate_pre = jnp.einsum(
        "sxcd,xdh->sxch", arrived_rows, gate_new, preferred_element_type=jnp.float32
    )
    up_pre = jnp.einsum("sxcd,xdh->sxch", arrived_rows, up_new, preferred_element_type=jnp.float32)
    hidden = (jax.nn.silu(gate_pre) * up_pre).astype(jnp.bfloat16)
    partial_value = jnp.einsum(
        "sxch,xhd->sxcd", hidden, down_new, preferred_element_type=jnp.float32
    )
    summed = lax.psum_scatter(
        partial_value.astype(jnp.bfloat16), "tp", scatter_dimension=3, tiled=True
    )
    returned = lax.all_to_all(summed, "fs", split_axis=0, concat_axis=0, tiled=True)
    returned_flat = returned.reshape(slots_all, returned.shape[3])
    pick_first = jnp.dot(select_first, returned_flat, preferred_element_type=jnp.float32)
    pick_second = jnp.dot(select_second, returned_flat, preferred_element_type=jnp.float32)
    mixed = route_weight[:, 0:1] * pick_first + route_weight[:, 1:2] * pick_second
    return (gate_new, up_new, down_new, mixed.astype(jnp.bfloat16))


def solution(mesh):
    return jax.shard_map(
        body,
        mesh=mesh,
        in_specs=(
            P(("gr", "fs"), "tp"),
            P(("gr", "fs")),
            P(None, ("gr", "fs"), "tp"),
            P(None, ("gr", "fs"), "tp"),
            P(None, ("gr", "fs"), "tp"),
            P(("gr", "fs"), None),
            P(("gr", "fs"), None),
        ),
        out_specs=(
            P("fs", None, "tp"),
            P("fs", None, "tp"),
            P("fs", "tp", None),
            P(("gr", "fs"), "tp"),
        ),
        check_vma=False,
    )
```

profile of v0, /device:TPU:15, one launch (start us, length us, event | category | flops | bytes accessed | tf_op | source)
XLA Modules:
  0.0 307.7 jit_solution(11874860149354385042)
XLA Ops:
  7.2 1.4 convert_element_type.48
  8.7 1.5 multiply_convert_fusion.1
  10.4 51.0 %all_to_all.45 = bf16[32,32,768]{2,1,0:T(8,128)(2,1)S(1)} all-to-all(bf16[32,32,768]{2,1,0:T(8,128)(2,1)S(1)} %pad_maximum_fusion), channel_id=1, replica_groups=mesh['gr'=2,'fs'=32,'tp'=8] {'fs'}, dimensions={0} | all-to-all | bytes 3145728 | tf_op jit(solution)/shard_map/all_to_all | solution.py:12
  61.5 1.4 pad_maximum_fusion.1
  62.9 0.9 copy-done.2
  64.6 7.0 %all-to-all-start.2 = ((f32[8,320,1]{1,2,0:T(1,128)}), f32[8,320,1]{1,2,0:T(1,128)S(1)}, u32[]{:S(2)}, u32[]{:S(2)}) async-start(f32[8,320,1]{1,2,0:T(1,128)} %broadcast_in_dim.2), calls=%async_computation.2 | async-start | bytes 24576 | tf_op jit(solution)/shard_map/all_to_all | solution.py:27
  72.0 1.5 reduce-window.6
  74.5 0.7 convolution_convert_fusion
  75.4 21.0 %all_to_all.46 = bf16[32,1,30,256]{3,2,1,0:T(8,128)(2,1)S(1)} all-to-all(bf16[32,1,30,256]{3,2,1,0:T(8,128)(2,1)S(1)} %bitcast.91), channel_id=1, replica_groups=mesh['gr'=2,'fs'=32,'tp'=8] {'fs'}, dimensions={0} | all-to-all | bytes 983040 | tf_op jit(solution)/shard_map/all_to_all | solution.py:69
  96.4 1.1 copy.72
  97.5 67.4 %all-gather.3.cloned.1.call-done = bf16[3,2048,256]{2,1,0:T(8,128)(2,1)} async-done(((bf16[3,1024,256]{2,1,0:T(8,128)(2,1)}), bf16[3,2048,256]{2,1,0:T(8,128)(2,1)}) %all-gather.3.cloned.1.call-update) | async-done | bytes 3145744 | tf_op jit(solution)/shard_map/all_gather | solution.py:22
  164.9 3.4 %fusion.54 = (bf16[1,2048,256]{2,1,0:T(8,128)(2,1)S(1)}, bf16[1,2048,256]{2,1,0:T(8,128)(2,1)}, bf16[1,2048,256]{2,1,0:T(8,128)(2,1)}) fusion(bf16[3,2048,256]{2,1,0:T(8,128)(2,1)} %all-gather.3.cloned.1.call-done), kind=kLoop, calls=%fused_computation.59 | loop fusion | bytes 6291456 | tf_op jit(solution)/shard_map/split | solution.py:22
  168.3 11.6 %copy.79 = bf16[1,2048,256]{2,0,1:T(2,128)(2,1)S(1)} copy(bf16[1,2048,256]{2,1,0:T(8,128)(2,1)S(1)} %get-tuple-element.16) | data formatting | bytes 2097152 | tf_op jit(solution)/shard_map/split | solution.py:22
  180.4 10.6 %reduce.11 = bf16[2048,256]{1,0:T(8,128)(2,1)S(1)} reduce(bf16[2048,1,256]{2,1,0:T(2,128)(2,1)S(1)} %bitcast.88, bf16[]{:T(256)} %broadcast.41), dimensions={1}, to_apply=%bitcast.83.reduce_sub_computation | reduce | bytes 2097154
  191.3 22.2 %all_to_all.47 = bf16[8,2,32768]{2,1,0:T(2,128)(2,1)S(1)} all-to-all(bf16[8,2,32768]{2,1,0:T(2,128)(2,1)S(1)} %reshape.88), channel_id=1, replica_groups=mesh['gr'=2,'fs'=32,'tp'=8] {'tp'}, dimensions={0} | all-to-all | bytes 2097152 | tf_op jit(solution)/shard_map/all_to_all | solution.py:45
  213.5 1.0 reshape.89
  215.9 4.6 %fusion.4 = f32[32,1,30,256]{3,0,2,1:T(8,128)} fusion(bf16[32,1,30,2048]{3,0,2,1:T(8,128)(2,1)} %all-gather.5.cloned.1.call-done, bf16[1,2048,256]{2,1,0:T(8,128)(2,1)} %get-tuple-element.18), kind=kOutput, calls=%fused_computation.7 | convolution fusion | flops 1006632960 | bytes 5963776 | tf_op jit(solution)/shard_map/sxcd,xdh->sxch/dot_general | solution.py:71
  220.6 8.4 %convert_bitcast_fusion = bf16[32,1,30,2048]{3,0,2,1:T(8,128)(2,1)} fusion(bf16[256,2048,1]{1,0,2:T(8,128)(2,1)S(1)} %reshape.81, bf16[32,1,30,2048]{3,0,2,1:T(8,128)(2,1)} %all-gather.5.cloned.1.call-done, bf16[1,2048,256]{2,1,0:T(8,128)(2,1)S(1)} %copy-done.1, f32[32,1,30,256]{3,0,2,1:T(8,128)} %fusion.4), kind=kOutput, calls=%fused_computation.4 | convolution fusion | flops 2016706560 | bytes 10944512 | tf_op jit(solution)/shard_map/sxch,xhd->sxcd/dot_general | solution.py:76
  229.0 40.6 %reduce-scatter.2.cloned.1.call-done = bf16[32,1,30,256]{3,0,2,1:T(8,128)(2,1)} async-done(((bf16[32,1,30,2048]{3,0,2,1:T(8,128)(2,1)}), bf16[32,1,30,256]{3,0,2,1:T(8,128)(2,1)}) %reduce-scatter.2.cloned.1.call-update) | async-done | bytes 491536 | tf_op jit(solution)/shard_map/reduce_scatter | solution.py:79
  269.6 2.1 copy.73
  271.7 10.1 %all-to-all-start.4 = ((bf16[32,1,30,256]{3,2,1,0:T(8,128)(2,1)}), bf16[32,1,30,256]{3,2,1,0:T(8,128)(2,1)S(1)}, u32[]{:S(2)}, u32[]{:S(2)}) async-start(bf16[32,1,30,256]{3,2,1,0:T(8,128)(2,1)} %copy.73), calls=%async_computation.5 | async-start | bytes 1048576 | tf_op jit(solution)/shard_map/all_to_all | solution.py:82
  282.4 1.4 copy.74
  283.8 15.8 %all-to-all-done.4 = bf16[32,1,30,256]{3,2,1,0:T(8,128)(2,1)S(1)} async-done(((bf16[32,1,30,256]{3,2,1,0:T(8,128)(2,1)}), bf16[32,1,30,256]{3,2,1,0:T(8,128)(2,1)S(1)}, u32[]{:S(2)}, u32[]{:S(2)}) %all-to-all-start.4) | async-done | bytes 491552 | tf_op jit(solution)/shard_map/all_to_all | solution.py:82
  300.1 1.1 fusion.26
  (46 shorter events, 6.0 us)
Async XLA Ops:
  7.2 1.4 copy-start.5
  7.2 1.5 copy-start
  7.2 157.7 %all-gather.3.cloned.1.call-start = ((), (), s32[]{:S(2)}) async-start(), calls=%async_computation.6 | async-start | bytes 4718592 | tf_op jit(solution)/shard_map/all_gather | solution.py:22
  62.9 0.9 copy-start.2
  62.9 8.7 %copy-start.3 = (s32[320,2]{0,1:T(2,128)S(1)}, s32[320,2]{0,1:T(2,128)}, u32[]{:S(2)}) copy-start(s32[320,2]{0,1:T(2,128)} %param.12) | copy-start | bytes 7684
  64.6 9.9 %all-to-all-start.2 = ((f32[8,320,1]{1,2,0:T(1,128)}), f32[8,320,1]{1,2,0:T(1,128)S(1)}, u32[]{:S(2)}, u32[]{:S(2)}) async-start(f32[8,320,1]{1,2,0:T(1,128)} %broadcast_in_dim.2), calls=%async_computation.2 | async-start | bytes 24576 | tf_op jit(solution)/shard_map/all_to_all | solution.py:27
  71.5 144.4 %all-gather.5.cloned.1.call-start = ((), (), s32[]{:S(2)}) async-start(), calls=%async_computation.7 | async-start | bytes 4423680 | tf_op jit(solution)/shard_map/all_gather | solution.py:70
  97.4 172.1 %reduce-scatter.2.cloned.1.call-start = ((), (), s32[]{:S(2)}) async-start(), calls=%async_computation.8 | async-start | bytes 4423680 | tf_op jit(solution)/shard_map/reduce_scatter | solution.py:79
  215.9 4.7 %copy-start.1 = (bf16[1,2048,256]{2,1,0:T(8,128)(2,1)S(1)}, bf16[1,2048,256]{2,1,0:T(8,128)(2,1)}, u32[]{:S(2)}) copy-start(bf16[1,2048,256]{2,1,0:T(8,128)(2,1)} %get-tuple-element.17) | copy-start | bytes 3145732
  228.9 52.8 %copy-start.4 = (f32[320,2]{0,1:T(2,128)S(1)}, f32[320,2]{0,1:T(2,128)}, u32[]{:S(2)}) copy-start(f32[320,2]{0,1:T(2,128)} %param.13) | copy-start | bytes 7684
  271.7 27.9 %all-to-all-start.4 = ((bf16[32,1,30,256]{3,2,1,0:T(8,128)(2,1)}), bf16[32,1,30,256]{3,2,1,0:T(8,128)(2,1)S(1)}, u32[]{:S(2)}, u32[]{:S(2)}) async-start(bf16[32,1,30,256]{3,2,1,0:T(8,128)(2,1)} %copy.73), calls=%async_computation.5 | async-start | bytes 1048576 | tf_op jit(solution)/shard_map/all_to_all | solution.py:82
Sparse Core Ops, SparseCore 0:
  63.0 101.8 all-gather.2
  167.6 46.1 all-gather.4
  229.1 40.4 reduce-scatter.1
where the time goes:
time: 308 us
  waiting for transfers between devices  124 us (40%)
  blocking collectives  94.2 us (31%)
  local copies, waits for them, and re-layouts  26.2 us (9%)
  starting transfers between devices  17.2 us (6%)
  other arithmetic  16.8 us (5%)
  matrix products  15.1 us (5%)
  between operations  14 us (5%)
    all_gather x1, waiting for transfers between devices, side_by_side_2(): lax.all_gather(both, axis, axis=dim, tiled=True)  67.4 us
    all_to_all x1, blocking collectives, side_by_side(): lax.all_to_all(both, axis, split_axis=split_dim, concat_axis=concat_dim,...  51 us
    reduce_scatter x1, waiting for transfers between devices, body(): lax.psum_scatter(partial_value.astype(jnp.bfloat16), 'tp', scatter_dimens...  40.6 us
    all_to_all x1, blocking collectives, body(): lax.all_to_all(down_rows, 'tp', split_axis=1, concat_axis=2, tiled=True)  22.2 us
    all_to_all x1, blocking collectives, body(): lax.all_to_all(outbound, 'fs', split_axis=0, concat_axis=0, tiled=True)  21 us
    all_to_all x1, waiting for transfers between devices, body(): lax.all_to_all(summed, 'fs', split_axis=0, concat_axis=0, tiled=True)  15.8 us
    split x2, local copies, waits for them, and re-layouts, side_by_side_2(): jnp.split(lax.all_gather(both, axis, axis=dim, tiled=True), ends, axis=al...  15 us
    unnamed x1, other arithmetic  10.6 us
  transfers between devices with their start and end apart: 5, of which 4 were waited for; matrix products, arithmetic and copies ran while one was open for 12% of the time, Pallas kernels for 0%

commit v1 on v0

--- a/solution.py
+++ b/solution.py
@@ -4,6 +4,18 @@
 from jax.sharding import PartitionSpec as P
 
 CAP = 30
+
+
+def choose_layers_all_on(mesh_name, a0):
+    return jnp.concatenate(
+        lax.all_to_all(
+            jnp.stack(jnp.split(a0, lax.axis_size(mesh_name), axis=1), axis=0),
+            axis_name=mesh_name,
+            concat_axis=0,
+            split_axis=0,
+        ),
+        axis=2,
+    )
 
 
 def side_by_side(arrays, axis, split_dim, concat_dim, along):
@@ -42,7 +54,7 @@
     down_cast = down_weight.astype(jnp.bfloat16)
     spread = side_by_side((gate_cast, up_cast, down_cast), "fs", 0, 1, 2)
     gate_new, up_new, down_rows = side_by_side_2((spread[0], spread[1], spread[2]), "gr", 1, 0)
-    down_new = lax.all_to_all(down_rows, "tp", split_axis=1, concat_axis=2, tiled=True)
+    down_new = choose_layers_all_on("tp", down_rows)
     values = prompt.astype(jnp.float32)
     tok_count = prompt.shape[0]
     col_width = prompt.shape[1]

time: 308 us -> 306 us (level)
  waiting for transfers between devices: 124 us -> 154 us
  blocking collectives: 94.2 us -> 71.9 us
  other arithmetic: 16.8 us -> 6.43 us
  starting transfers between devices: 17.2 us -> 22.4 us
  local copies, waits for them, and re-layouts: 26.2 us -> 22.3 us
    all_to_all x1 -> x0, blocking collectives: 22.2 us -> none  [body(): lax.all_to_all(down_rows, 'tp', split_axis=1, concat_axis=2, tiled=True)]
    all_to_all x0 -> x1, waiting for transfers between devices: none -> 18.5 us  [choose_layers_all_on(): lax.all_to_all(jnp.stack(jnp.split(a0, lax.axis_size(mesh_name), axis=1),...]
    split x2 -> x1, local copies, waits for them, and re-layouts: 15 us -> 2.65 us  [side_by_side_2(): jnp.split(lax.all_gather(both, axis, axis=dim, tiled=True), ends, axis=al...]
    unnamed x1 -> x0, other arithmetic: 10.6 us -> none
    all_gather x1, waiting for transfers between devices: 0.02 us -> 8.38 us  [body(): arrived_rows = lax.all_gather(moved_cols, 'tp', axis=3, tiled=True)]
    unnamed x18 -> x17, local copies, waits for them, and re-layouts: 4.59 us -> 12.5 us
    all_to_all x0 -> x1, starting transfers between devices: none -> 5.28 us  [choose_layers_all_on(): lax.all_to_all(jnp.stack(jnp.split(a0, lax.axis_size(mesh_name), axis=1),...]
  transfers between devices with their start and end apart: 5 -> 6, of which waited for: 4 -> 6; matrix products, arithmetic and copies ran while one was open for 12% -> 7% of each run, Pallas kernels for 0% -> 0%
where the time goes in v1:
time: 306 us; the launch traced here: 305 us
  waiting for transfers between devices  154 us (50%)
  blocking collectives  71.9 us (23%)
  starting transfers between devices  22.4 us (7%)
  local copies, waits for them, and re-layouts  22.3 us (7%)
  matrix products  13.9 us (5%)
  between operations  13.9 us (5%)
  other arithmetic  6.43 us (2%)
    all_gather x1, waiting for transfers between devices, side_by_side_2(): lax.all_gather(both, axis, axis=dim, tiled=True)  67.4 us
    all_to_all x1, blocking collectives, side_by_side(): lax.all_to_all(both, axis, split_axis=split_dim, concat_axis=concat_dim,...  51 us
    reduce_scatter x1, waiting for transfers between devices, body(): lax.psum_scatter(partial_value.astype(jnp.bfloat16), 'tp', scatter_dimens...  43.4 us
    all_to_all x1, blocking collectives, body(): lax.all_to_all(outbound, 'fs', split_axis=0, concat_axis=0, tiled=True)  20.9 us
    all_to_all x1, waiting for transfers between devices, choose_layers_all_on(): lax.all_to_all(jnp.stack(jnp.split(a0, lax.axis_size(mesh_name), axis=1),...  18.5 us
    all_to_all x1, waiting for transfers between devices, body(): lax.all_to_all(summed, 'fs', split_axis=0, concat_axis=0, tiled=True)  16.3 us
    unnamed x17, local copies, waits for them, and re-layouts  12.5 us
    all_to_all x1, starting transfers between devices, body(): lax.all_to_all(summed, 'fs', split_axis=0, concat_axis=0, tiled=True)  10.1 us
  transfers between devices with their start and end apart: 6, of which 6 were waited for; matrix products, arithmetic and copies ran while one was open for 7% of the time, Pallas kernels for 0%

profile of v1, /device:TPU:15, one launch (start us, length us, event | category | flops | bytes accessed | tf_op | source)
XLA Modules:
  0.0 305.2 jit_solution(2975324531599720272)
XLA Ops:
  8.5 1.9 multiply_convert_fusion.1
  10.5 51.0 %all_to_all.32 = bf16[32,32,768]{2,1,0:T(8,128)(2,1)S(1)} all-to-all(bf16[32,32,768]{2,1,0:T(8,128)(2,1)S(1)} %pad_maximum_fusion), channel_id=1, replica_groups=mesh['gr'=2,'fs'=32,'tp'=8] {'fs'}, dimensions={0} | all-to-all | bytes 3145728 | tf_op jit(solution)/shard_map/all_to_all | solution.py:24
  63.8 7.0 %all-to-all-start.2 = ((f32[8,320,1]{1,2,0:T(1,128)}), f32[8,320,1]{1,2,0:T(1,128)S(1)}, u32[]{:S(2)}, u32[]{:S(2)}) async-start(f32[8,320,1]{1,2,0:T(1,128)} %broadcast_in_dim.2), calls=%async_computation.2 | async-start | bytes 24576 | tf_op jit(solution)/shard_map/all_to_all | solution.py:39
  71.3 1.5 reduce-window.6
  74.6 20.9 %all_to_all.33 = bf16[32,1,30,256]{3,2,1,0:T(8,128)(2,1)S(1)} all-to-all(bf16[32,1,30,256]{3,2,1,0:T(8,128)(2,1)S(1)} %bitcast.116), channel_id=1, replica_groups=mesh['gr'=2,'fs'=32,'tp'=8] {'fs'}, dimensions={0} | all-to-all | bytes 983040 | tf_op jit(solution)/shard_map/all_to_all | solution.py:81
  96.7 67.4 %all-gather.3.cloned.1.call-done = bf16[3,2048,256]{2,1,0:T(8,128)(2,1)} async-done(((bf16[3,1024,256]{2,1,0:T(8,128)(2,1)}), bf16[3,2048,256]{2,1,0:T(8,128)(2,1)}) %all-gather.3.cloned.1.call-update) | async-done | bytes 3145744 | tf_op jit(solution)/shard_map/all_gather | solution.py:34
  164.1 1.6 fusion.56
  165.7 1.6 fusion.55
  167.2 1.6 fusion.54
  168.8 1.6 fusion.53
  170.4 1.6 fusion.52
  171.9 1.6 fusion.51
  173.5 1.6 fusion.50
  175.1 1.6 fusion.49
  176.6 5.3 %all-to-all-start.1 = ((bf16[8,1,256,256]{3,2,1,0:T(8,128)(2,1)}), bf16[8,1,256,256]{3,2,1,0:T(8,128)(2,1)S(1)}, u32[]{:S(2)}, u32[]{:S(2)}) async-start(bf16[8,1,256,256]{3,2,1,0:T(8,128)(2,1)} %fusion.49), calls=%async_computation.1 | async-start | bytes 2097152 | tf_op jit(solution)/shard_map/all_to_all | solution.py:11
  181.9 2.7 fusion.62
  184.6 18.5 %all-to-all-done.1 = bf16[8,1,256,256]{3,2,1,0:T(8,128)(2,1)S(1)} async-done(((bf16[8,1,256,256]{3,2,1,0:T(8,128)(2,1)}), bf16[8,1,256,256]{3,2,1,0:T(8,128)(2,1)S(1)}, u32[]{:S(2)}, u32[]{:S(2)}) %all-to-all-start.1) | async-done | bytes 1048608 | tf_op jit(solution)/shard_map/all_to_all | solution.py:11
  203.6 8.4 %all-gather.5.cloned.1.call-done = bf16[32,1,30,2048]{3,0,2,1:T(8,128)(2,1)} async-done(((bf16[32,1,30,256]{3,0,2,1:T(8,128)(2,1)}), bf16[32,1,30,2048]{3,0,2,1:T(8,128)(2,1)}) %all-gather.5.cloned.1.call-update) | async-done | bytes 3932176 | tf_op jit(solution)/shard_map/all_gather | solution.py:82
  211.9 3.6 %fusion.4 = f32[32,1,30,256]{3,0,2,1:T(8,128)S(1)} fusion(bf16[32,1,30,2048]{3,0,2,1:T(8,128)(2,1)} %all-gather.5.cloned.1.call-done, bf16[1,2048,256]{2,1,0:T(8,128)(2,1)} %get-tuple-element.25), kind=kOutput, calls=%fused_computation.7 | convolution fusion | flops 1006632960 | bytes 5963776 | tf_op jit(solution)/shard_map/sxcd,xdh->sxch/dot_general | solution.py:83
  215.6 8.1 %convert_bitcast_fusion = bf16[32,1,30,2048]{3,0,2,1:T(8,128)(2,1)} fusion(bf16[256,2048,1]{0,1,2:T(8,128)(2,1)S(1)} %bitcast.113, bf16[32,1,30,2048]{3,0,2,1:T(8,128)(2,1)} %all-gather.5.cloned.1.call-done, bf16[1,2048,256]{2,1,0:T(8,128)(2,1)S(1)} %get-tuple-element.24, f32[32,1,30,256]{3,0,2,1:T(8,128)S(1)} %fusion.4), kind=kOutput, calls=%fused_computation.4 | convolution fusion | flops 2016706560 | bytes 10944512 | tf_op jit(solution)/shard_map/sxch,xhd->sxcd/dot_general | solution.py:88
  223.7 43.4 %reduce-scatter.2.cloned.1.call-done = bf16[32,1,30,256]{3,0,2,1:T(8,128)(2,1)} async-done(((bf16[32,1,30,2048]{3,0,2,1:T(8,128)(2,1)}), bf16[32,1,30,256]{3,0,2,1:T(8,128)(2,1)}) %reduce-scatter.2.cloned.1.call-update) | async-done | bytes 491536 | tf_op jit(solution)/shard_map/reduce_scatter | solution.py:91
  267.1 2.1 copy.55
  269.2 10.1 %all-to-all-start.4 = ((bf16[32,1,30,256]{3,2,1,0:T(8,128)(2,1)}), bf16[32,1,30,256]{3,2,1,0:T(8,128)(2,1)S(1)}, u32[]{:S(2)}, u32[]{:S(2)}) async-start(bf16[32,1,30,256]{3,2,1,0:T(8,128)(2,1)} %copy.55), calls=%async_computation.5 | async-start | bytes 1048576 | tf_op jit(solution)/shard_map/all_to_all | solution.py:94
  280.8 16.3 %all-to-all-done.4 = bf16[32,1,30,256]{3,2,1,0:T(8,128)(2,1)S(1)} async-done(((bf16[32,1,30,256]{3,2,1,0:T(8,128)(2,1)}), bf16[32,1,30,256]{3,2,1,0:T(8,128)(2,1)S(1)}, u32[]{:S(2)}, u32[]{:S(2)}) %all-to-all-start.4) | async-done | bytes 491552 | tf_op jit(solution)/shard_map/all_to_all | solution.py:94
  (43 shorter events, 10.7 us)
Async XLA Ops:
  7.2 156.9 %all-gather.3.cloned.1.call-start = ((), (), s32[]{:S(2)}) async-start(), calls=%async_computation.6 | async-start | bytes 4718592 | tf_op jit(solution)/shard_map/all_gather | solution.py:34
  61.7 1.4 copy-start.1
  61.7 9.1 %copy-start.2 = (s32[320,2]{0,1:T(2,128)S(1)}, s32[320,2]{0,1:T(2,128)}, u32[]{:S(2)}) copy-start(s32[320,2]{0,1:T(2,128)} %param.12) | copy-start | bytes 7684
  63.8 9.9 %all-to-all-start.2 = ((f32[8,320,1]{1,2,0:T(1,128)}), f32[8,320,1]{1,2,0:T(1,128)S(1)}, u32[]{:S(2)}, u32[]{:S(2)}) async-start(f32[8,320,1]{1,2,0:T(1,128)} %broadcast_in_dim.2), calls=%async_computation.2 | async-start | bytes 24576 | tf_op jit(solution)/shard_map/all_to_all | solution.py:39
  70.8 141.1 %all-gather.5.cloned.1.call-start = ((), (), s32[]{:S(2)}) async-start(), calls=%async_computation.7 | async-start | bytes 4423680 | tf_op jit(solution)/shard_map/all_gather | solution.py:82
  176.6 26.4 %all-to-all-start.1 = ((bf16[8,1,256,256]{3,2,1,0:T(8,128)(2,1)}), bf16[8,1,256,256]{3,2,1,0:T(8,128)(2,1)S(1)}, u32[]{:S(2)}, u32[]{:S(2)}) async-start(bf16[8,1,256,256]{3,2,1,0:T(8,128)(2,1)} %fusion.49), calls=%async_computation.1 | async-start | bytes 2097152 | tf_op jit(solution)/shard_map/all_to_all | solution.py:11
  181.9 85.2 %reduce-scatter.2.cloned.1.call-start = ((), (), s32[]{:S(2)}) async-start(), calls=%async_computation.8 | async-start | bytes 4423680 | tf_op jit(solution)/shard_map/reduce_scatter | solution.py:91
  184.6 31.0 %copy-start = (bf16[1,2048,256]{2,1,0:T(8,128)(2,1)}, bf16[1,2048,256]{2,1,0:T(8,128)(2,1)S(1)}, u32[]{:S(2)}) copy-start(bf16[1,2048,256]{2,1,0:T(8,128)(2,1)S(1)} %get-tuple-element.24) | copy-start | bytes 3145732
  223.7 55.7 %copy-start.3 = (f32[320,2]{0,1:T(2,128)S(1)}, f32[320,2]{0,1:T(2,128)}, u32[]{:S(2)}) copy-start(f32[320,2]{0,1:T(2,128)} %param.13) | copy-start | bytes 7684
  269.2 27.9 %all-to-all-start.4 = ((bf16[32,1,30,256]{3,2,1,0:T(8,128)(2,1)}), bf16[32,1,30,256]{3,2,1,0:T(8,128)(2,1)S(1)}, u32[]{:S(2)}, u32[]{:S(2)}) async-start(bf16[32,1,30,256]{3,2,1,0:T(8,128)(2,1)} %copy.55), calls=%async_computation.5 | async-start | bytes 1048576 | tf_op jit(solution)/shard_map/all_to_all | solution.py:94
Sparse Core Ops, SparseCore 0:
  63.2 100.8 all-gather.2
  166.2 45.6 all-gather.4
  223.8 43.2 reduce-scatter.1
